TPU v7x, 32 devices: a whole 2x2x4 slice. The times are simulated.
32 devices in a mesh: rep: 2 (over x), fs: 8 (over z, y), tp: 2 (over core).
Axes of the slice: x: 2, y: 2, z: 4, core: 2. Of those that a mesh axis runs over, the one named last changes fastest.
Arguments:
- tokens: bfloat16 [5120, 2048], P(('rep', 'fs'), 'tp'), may hold values from -30 to 30
- mixer_gain: float32 [2048], P('tp'), may hold values from 0.1 to 1.9
- outer_weight: float32 [2048, 1024], P('fs', 'tp'), may hold values from -0.125 to 0.125
- inner_weight: float32 [2048, 1024], P('fs', 'tp'), may hold values from -0.125 to 0.125
- value_weight: float32 [2048, 1024], P('fs', 'tp'), may hold values from -0.125 to 0.125
- outer_scale: float32 [1024], P(('tp', 'fs')), may hold values from 0.5 to 2
- inner_scale: float32 [1024], P(('tp', 'fs')), may hold values from 0.5 to 2
- value_scale: float32 [1024], P(('tp', 'fs')), may hold values from 0.5 to 2
- mixer_taps: float32 [3, 1024], P(None, 'tp'), may hold values from -3.5 to 3.5
- mixer_project: float32 [1024, 2048], P('tp', 'fs'), may hold values from -0.1875 to 0.1875
- project_scale: float32 [2048], P('fs'), may hold values from 0.5 to 2
- channel_gain: float32 [2048], P('tp'), may hold values from 0.1 to 1.9
- gate_weight: float32 [2048, 5632], P('fs', 'tp'), may hold values from -0.125 to 0.125
- gate_scale: float32 [5632], P(('tp', 'fs')), may hold values from 0.5 to 2
- up_weight: float32 [2048, 5632], P('fs', 'tp'), may hold values from -0.125 to 0.125
- up_scale: float32 [5632], P(('tp', 'fs')), may hold values from 0.5 to 2
- channel_taps: float32 [3, 5632], P(None, 'tp'), may hold values from -3.5 to 3.5
- channel_bias: float32 [5632], P('tp'), may hold values from -3 to 3
- down_weight: float32 [5632, 2048], P('tp', 'fs'), may hold values from -0.078125 to 0.078125
- down_scale: float32 [2048], P('fs'), may hold values from 0.5 to 2
Outputs:
- result: bfloat16 [5120, 2048], P(('rep', 'fs'), 'tp')
All inputs are finite; a program needn't handle non-finite values.
Results may differ from a plain program's by a relative error of at most 0.015.
Values may be sent and summed in bfloat16 or wider, within the bound.
A program may use at most 128 MiB of HBM per device.

v0:
```python
import jax
import jax.numpy as jnp
from jax import lax
from jax.sharding import PartitionSpec as P

LEN = 320
epsilon = 1e-06


def normalize(token_rows, gain):
    values = token_rows.astype(jnp.float32)
    squares = lax.psum(jnp.sum(values * values, axis=1), "tp")
    features = values.shape[1] * lax.axis_size("tp")
    inverse = lax.rsqrt(squares / features + epsilon)
    local = (values * inverse[:, None] * gain).astype(jnp.bfloat16)
    return lax.all_gather(local, "tp", axis=1, tiled=True)


def causal_taps(values, taps):
    tap_count = taps.shape[0]
    grouped = values.reshape(-1, LEN, values.shape[1])
    padded = jnp.pad(grouped, ((0, 0), (tap_count - 1, 0), (0, 0)))
    running = jnp.zeros_like(grouped)
    for offset in range(tap_count):
        running = running + taps[offset] * padded[:, offset : offset + LEN]
    return running.reshape(values.shape)


def accumulate(whole, pieces):
    return tuple(
        (
            jnp.dot(whole, weight_block, preferred_element_type=jnp.float32)
            for weight_block in pieces
        )
    )


def project_back(hidden, weight, scale):
    product = (
        jnp.dot(
            hidden,
            lax.all_gather(weight, "fs", axis=1, tiled=True),
            preferred_element_type=jnp.float32,
        )
        * scale
    )
    partials = lax.optimization_barrier(product.astype(jnp.bfloat16)).astype(jnp.float32)
    return lax.psum_scatter(
        partials.astype(jnp.bfloat16), "tp", scatter_dimension=1, tiled=True
    ).astype(jnp.float32)


def per_device(
    tokens,
    mixer_gain,
    outer_weight,
    inner_weight,
    value_weight,
    outer_scale,
    inner_scale,
    value_scale,
    mixer_taps,
    mixer_project,
    project_scale,
    channel_gain,
    gate_weight,
    gate_scale,
    up_weight,
    up_scale,
    channel_taps,
    channel_bias,
    down_weight,
    down_scale,
):
    outer_full, inner_full, value_full, gate_full, up_full, project_full, down_full = (
        lax.all_gather(outer_scale, "fs", axis=0, tiled=True),
        lax.all_gather(inner_scale, "fs", axis=0, tiled=True),
        lax.all_gather(value_scale, "fs", axis=0, tiled=True),
        lax.all_gather(gate_scale, "fs", axis=0, tiled=True),
        lax.all_gather(up_scale, "fs", axis=0, tiled=True),
        lax.all_gather(project_scale, "fs", axis=0, tiled=True),
        lax.all_gather(down_scale, "fs", axis=0, tiled=True),
    )
    channel_low = (gate_weight.astype(jnp.bfloat16), up_weight.astype(jnp.bfloat16))
    normed = normalize(tokens, mixer_gain)
    mixer_low = (
        outer_weight.astype(jnp.bfloat16),
        inner_weight.astype(jnp.bfloat16),
        value_weight.astype(jnp.bfloat16),
    )
    outer_part, inner_part, value_part = accumulate(
        normed,
        (
            lax.all_gather(mixer_low[0], "fs", axis=0, tiled=True),
            lax.all_gather(mixer_low[1], "fs", axis=0, tiled=True),
            lax.all_gather(mixer_low[2], "fs", axis=0, tiled=True),
        ),
    )
    outer_part = outer_part * outer_full
    conv_input = inner_part * inner_full * (value_part * value_full)
    mixed = (outer_part * causal_taps(conv_input, mixer_taps)).astype(jnp.bfloat16)
    mixer_sum = project_back(mixed, mixer_project.astype(jnp.bfloat16), project_full)
    middle = (tokens.astype(jnp.float32) + mixer_sum).astype(jnp.bfloat16)
    normed_two = normalize(middle, channel_gain)
    gate_part, up_part = accumulate(
        normed_two,
        (
            lax.all_gather(channel_low[0], "fs", axis=0, tiled=True),
            lax.all_gather(channel_low[1], "fs", axis=0, tiled=True),
        ),
    )
    gate_part = gate_part * gate_full
    up_part = up_part * up_full
    hidden = (jax.nn.silu(causal_taps(gate_part, channel_taps) + channel_bias) * up_part).astype(
        jnp.bfloat16
    )
    channel_sum = project_back(hidden, down_weight.astype(jnp.bfloat16), down_full)
    return (middle.astype(jnp.float32) + channel_sum).astype(jnp.bfloat16)


def solution(mesh):
    placed = (
        P(("rep", "fs"), "tp"),
        P("tp"),
        P("fs", "tp"),
        P("fs", "tp"),
        P("fs", "tp"),
        P(("tp", "fs")),
        P(("tp", "fs")),
        P(("tp", "fs")),
        P(None, "tp"),
        P("tp", "fs"),
        P("fs"),
        P("tp"),
        P("fs", "tp"),
        P(("tp", "fs")),
        P("fs", "tp"),
        P(("tp", "fs")),
        P(None, "tp"),
        P("tp"),
        P("tp", "fs"),
        P("fs"),
    )
    return jax.shard_map(
        per_device, mesh=mesh, in_specs=placed, out_specs=P(("rep", "fs"), "tp"), check_vma=False
    )
```

profile of v0, /device:TPU:0, one launch (start us, length us, event | category | flops | bytes accessed | tf_op | source)
XLA Modules:
  0.0 787.0 jit_solution(13122378445534658382)
XLA Ops:
  6.5 1.4 fusion.4
  7.9 2.8 psum.14
  10.7 2.1 fusion.6
  13.0 0.0 all-gather.16.cloned.1.call-start
  13.0 0.7 convert_element_type.70
  13.8 0.0 all-gather.18.cloned.1.call-start
  13.9 0.7 convert_element_type.71
  14.6 0.0 all-gather.14.cloned.1.call-start
  14.7 0.7 convert_element_type.69
  15.5 0.0 all-gather.20.cloned.1.call-start
  15.5 0.7 convert_element_type.73
  16.3 0.0 reduce-scatter.3.cloned.1.call-start
  16.4 0.7 dynamic-slice
  18.4 0.2 dynamic-update-slice
  18.6 0.2 dynamic-update-slice.1
  18.9 0.2 dynamic-update-slice.2
  19.1 0.3 dynamic-update-slice.3
  19.4 0.3 dynamic-update-slice.4
  19.6 39.4 %all-reduce.7 = (f32[512]{0:T(512)S(1)}, f32[512]{0:T(512)S(1)}, f32[512]{0:T(512)S(1)}, f32[2816]{0:T(1024)}, f32[2816]{0:T(1024)}) all-reduce(f32[512]{0:T(512)S(1)} %dynamic-update-slice.1, f32[512]{0:T(512)S(1)} %dynamic-update-slice.2, f32[512]{0:T(512)S(1)} %dynamic-update-slice, ...), channel_id=1, replica_groups=mesh['rep'=2,'fs'=8,'tp'=2] {'fs'}, use_global_device_ids=true, to_apply=%add.3 | all-reduce | flops 7168 | bytes 57344
  59.0 16.7 %all-gather = f32[8,1,256]{2,1,0:T(1,128)S(1)} all-gather(f32[1,1,256]{2,1,0:T(1,128)S(1)} %bitcast.52), channel_id=1, replica_groups=mesh['rep'=2,'fs'=8,'tp'=2] {'fs'}, dimensions={0}, use_global_device_ids=true | all-gather | bytes 9216 | tf_op jit(solution)/shard_map/all_gather | solution.py:81
  75.8 1.8 all-gather.16.cloned.1.call-done
  77.6 2.9 convolution_multiply_fusion.5
  80.5 46.9 %all-gather.18.cloned.1.call-done = bf16[2048,512]{1,0:T(8,128)(2,1)} async-done(((bf16[256,512]{1,0:T(8,128)(2,1)}), bf16[2048,512]{1,0:T(8,128)(2,1)}) %all-gather.18.cloned.1.call-update) | async-done | bytes 2097168 | tf_op jit(solution)/shard_map/all_gather | solution.py:96
  127.4 2.5 fusion.12
  129.9 47.2 %all-gather.14.cloned.1.call-done = bf16[2048,512]{1,0:T(8,128)(2,1)} async-done(((bf16[256,512]{1,0:T(8,128)(2,1)}), bf16[2048,512]{1,0:T(8,128)(2,1)}) %all-gather.14.cloned.1.call-update) | async-done | bytes 2097168 | tf_op jit(solution)/shard_map/all_gather | solution.py:94
  177.0 50.8 %all-gather.20.cloned.1.call-done = bf16[512,2048]{1,0:T(8,128)(2,1)} async-done(((bf16[512,256]{1,0:T(8,128)(2,1)}), bf16[512,2048]{1,0:T(8,128)(2,1)}) %all-gather.20.cloned.1.call-update) | async-done | bytes 2097168 | tf_op jit(solution)/shard_map/all_gather | solution.py:42
  227.8 5.1 fusion.2
  233.0 0.0 all-gather.22.cloned.1.call-start
  233.0 6.9 reduce-scatter.3.cloned.1.call-done
  239.9 1.4 fusion.8
  241.3 2.5 psum.15
  243.8 2.2 fusion.10
  246.0 0.0 all-gather.24.cloned.1.call-start
  246.1 1.2 convert_element_type.79
  247.3 0.0 all-gather.26.cloned.1.call-start
  247.4 3.2 convert_element_type.80
  250.6 0.0 all-gather.28.cloned.1.call-start
  250.7 1.2 convert_element_type.82
  251.9 0.0 reduce-scatter.5.cloned.1.call-start
  252.0 21.1 %all-gather.1 = f32[8,1,256]{2,1,0:T(1,128)S(1)} all-gather(f32[1,1,256]{2,1,0:T(1,128)S(1)} %bitcast.53), channel_id=1, replica_groups=mesh['rep'=2,'fs'=8,'tp'=2] {'fs'}, dimensions={0}, use_global_device_ids=true | all-gather | bytes 9216 | tf_op jit(solution)/shard_map/all_gather | solution.py:82
  273.1 1.0 slice_reduce_fusion.2
  274.1 149.5 %all-gather.24.cloned.1.call-done = bf16[2048,2816]{1,0:T(8,128)(2,1)} async-done(((bf16[256,2816]{1,0:T(8,128)(2,1)}), bf16[2048,2816]{1,0:T(8,128)(2,1)}) %all-gather.24.cloned.1.call-update) | async-done | bytes 11534352 | tf_op jit(solution)/shard_map/all_gather | solution.py:108
  423.6 10.5 %convolution_multiply_fusion.1 = f32[320,2816]{1,0:T(8,128)} fusion(bf16[320,2048]{1,0:T(8,128)(2,1)} %all-gather.22.cloned.1.call-done, bf16[2048,2816]{1,0:T(8,128)(2,1)} %all-gather.24.cloned.1.call-done, f32[2816]{0:T(1024)S(1)} %copy-done.18), kind=kOutput, calls=%fused_computation.2 | convolution fusion | flops 3691888640 | bytes 16460800 | tf_op jit(solution)/shard_map/dot_general | solution.py:32
  434.1 153.2 %all-gather.26.cloned.1.call-done = bf16[2048,2816]{1,0:T(8,128)(2,1)} async-done(((bf16[256,2816]{1,0:T(8,128)(2,1)}), bf16[2048,2816]{1,0:T(8,128)(2,1)}) %all-gather.26.cloned.1.call-update) | async-done | bytes 11534352 | tf_op jit(solution)/shard_map/all_gather | solution.py:109
  587.3 163.4 %all-gather.28.cloned.1.call-done = bf16[2816,2048]{1,0:T(8,128)(2,1)} async-done(((bf16[2816,256]{1,0:T(8,128)(2,1)}), bf16[2816,2048]{1,0:T(8,128)(2,1)}) %all-gather.28.cloned.1.call-update) | async-done | bytes 11534352 | tf_op jit(solution)/shard_map/all_gather | solution.py:42
  750.7 20.5 %fusion.3 = bf16[320,2048]{1,0:T(8,128)(2,1)} fusion(bf16[2816,2048]{1,0:T(8,128)(2,1)} %all-gather.28.cloned.1.call-done, f32[2048]{0:T(1024)S(1)} %bitcast.48, bf16[320,2048]{1,0:T(8,128)(2,1)S(1)} %copy-done.15, bf16[2048,2816]{1,0:T(8,128)(2,1)} %all-gather.26.cloned.1.call-done, f32[320,2816]{1,0:T(8,128)} %convolution_multiply_fusion.1, ...), kind=kOutput, calls=%fused_computation.9 | convolution fusion | flops 7395000320 | bytes 32963584 | tf_op jit(solution)/shard_map/dot_general | solution.py:40
  771.3 6.9 reduce-scatter.5.cloned.1.call-done
  778.2 2.3 fusion.11
  (68 shorter events, 0.4 us)
Async XLA Ops:
  6.5 6.5 copy-start.4
  6.5 7.3 copy-start.5
  6.5 69.2 %all-gather.12.cloned.1.call-start = ((), (), s32[]{:S(2)}) async-start(), calls=%async_computation.2 | async-start | bytes 1966080 | tf_op jit(solution)/shard_map/all_gather | solution.py:16
  7.9 6.7 copy-start.6
  12.9 2.7 copy-start.7
  12.9 3.5 copy-start.22
  12.9 5.5 copy-start.19
  12.9 5.7 copy-start.20
  12.9 5.9 copy-start.21
  12.9 6.2 copy-start.10
  12.9 6.4 copy-start.11
  13.0 46.0 %copy-start.12 = (f32[256]{0:T(256)S(1)}, f32[256]{0:T(256)}, u32[]{:S(2)}) copy-start(f32[256]{0:T(256)} %param.30) | copy-start | bytes 3076
  13.0 62.8 %copy-start.8 = (f32[3,512]{1,0:T(4,128)S(1)}, f32[3,512]{1,0:T(4,128)}, u32[]{:S(2)}) copy-start(f32[3,512]{1,0:T(4,128)} %param.28) | copy-start | bytes 18436
  13.0 64.6 %all-gather.16.cloned.1.call-start = ((), (), s32[]{:S(2)}) async-start(), calls=%async_computation.4 | async-start | bytes 2359296 | tf_op jit(solution)/shard_map/all_gather | solution.py:95
  13.8 113.6 %all-gather.18.cloned.1.call-start = ((), (), s32[]{:S(2)}) async-start(), calls=%async_computation.5 | async-start | bytes 2359296 | tf_op jit(solution)/shard_map/all_gather | solution.py:96
  14.6 162.4 %all-gather.14.cloned.1.call-start = ((), (), s32[]{:S(2)}) async-start(), calls=%async_computation.3 | async-start | bytes 2359296 | tf_op jit(solution)/shard_map/all_gather | solution.py:94
  15.5 212.4 %all-gather.20.cloned.1.call-start = ((), (), s32[]{:S(2)}) async-start(), calls=%async_computation.6 | async-start | bytes 2359296 | tf_op jit(solution)/shard_map/all_gather | solution.py:42
  16.3 223.6 %reduce-scatter.3.cloned.1.call-start = ((), (), s32[]{:S(2)}) async-start(), calls=%async_computation.7 | async-start | bytes 1966080 | tf_op jit(solution)/shard_map/reduce_scatter | solution.py:48
  77.6 49.8 %copy-start.14 = (bf16[320,2048]{1,0:T(8,128)(2,1)S(1)}, bf16[320,2048]{1,0:T(8,128)(2,1)}, u32[]{:S(2)}) copy-start(bf16[320,2048]{1,0:T(8,128)(2,1)} %all-gather.12.cloned.1.call-done) | copy-start | bytes 3932164
  227.8 12.1 %copy-start = (bf16[320,1024]{1,0:T(8,128)(2,1)S(1)}, bf16[320,1024]{1,0:T(8,128)(2,1)}, u32[]{:S(2)}) copy-start(bf16[320,1024]{1,0:T(8,128)(2,1)} %param.20) | copy-start | bytes 1966084
  232.9 10.8 %copy-start.9 = (f32[1024]{0:T(1024)S(1)}, f32[1024]{0:T(1024)}, u32[]{:S(2)}) copy-start(f32[1024]{0:T(1024)} %param.31) | copy-start | bytes 12292
  233.0 13.1 %copy-start.2 = (f32[256,2816]{1,0:T(8,128)S(1)}, f32[256,2816]{1,0:T(8,128)}, u32[]{:S(2)}) copy-start(f32[256,2816]{1,0:T(8,128)} %param.32) | copy-start | bytes 8650756
  233.0 41.1 %all-gather.22.cloned.1.call-start = ((), (), s32[]{:S(2)}) async-start(), calls=%async_computation.8 | async-start | bytes 1966080 | tf_op jit(solution)/shard_map/all_gather | solution.py:16
  246.0 177.6 %all-gather.24.cloned.1.call-start = ((), (), s32[]{:S(2)}) async-start(), calls=%async_computation.9 | async-start | bytes 12976128 | tf_op jit(solution)/shard_map/all_gather | solution.py:108
  247.3 3.4 copy-start.3
  247.3 340.0 %all-gather.26.cloned.1.call-start = ((), (), s32[]{:S(2)}) async-start(), calls=%async_computation.10 | async-start | bytes 12976128 | tf_op jit(solution)/shard_map/all_gather | solution.py:109
  250.6 1.4 copy-start.13
  250.6 173.0 %copy-start.18 = (f32[2816]{0:T(1024)S(1)}, f32[2816]{0:T(1024)}, u32[]{:S(2)}) copy-start(f32[2816]{0:T(1024)} %get-tuple-element.11) | copy-start | bytes 33796
  250.6 500.1 %all-gather.28.cloned.1.call-start = ((), (), s32[]{:S(2)}) async-start(), calls=%async_computation.11 | async-start | bytes 12976128 | tf_op jit(solution)/shard_map/all_gather | solution.py:42
  251.9 526.3 %reduce-scatter.5.cloned.1.call-start = ((), (), s32[]{:S(2)}) async-start(), calls=%async_computation.12 | async-start | bytes 1966080 | tf_op jit(solution)/shard_map/reduce_scatter | solution.py:48
  423.6 327.1 %copy-start.15 = (bf16[320,2048]{1,0:T(8,128)(2,1)S(1)}, bf16[320,2048]{1,0:T(8,128)(2,1)}, u32[]{:S(2)}) copy-start(bf16[320,2048]{1,0:T(8,128)(2,1)} %all-gather.22.cloned.1.call-done) | copy-start | bytes 3932164
  423.6 327.1 %copy-start.16 = (f32[2816]{0:T(1024)S(1)}, f32[2816]{0:T(1024)}, u32[]{:S(2)}) copy-start(f32[2816]{0:T(1024)} %param.37) | copy-start | bytes 33796
  423.6 327.1 %copy-start.17 = (f32[2816]{0:T(1024)S(1)}, f32[2816]{0:T(1024)}, u32[]{:S(2)}) copy-start(f32[2816]{0:T(1024)} %get-tuple-element.12) | copy-start | bytes 33796
  750.7 27.5 %copy-start.1 = (bf16[320,1024]{1,0:T(8,128)(2,1)S(1)}, bf16[320,1024]{1,0:T(8,128)(2,1)}, u32[]{:S(2)}) copy-start(bf16[320,1024]{1,0:T(8,128)(2,1)} %reduce-scatter.3.cloned.1.call-done) | copy-start | bytes 1966084
Sparse Core Ops, SparseCore 0:
  13.0 11.9 all-gather.11
  27.1 50.3 all-gather.15
  79.7 47.6 all-gather.17
  129.4 47.6 all-gather.13
  178.9 48.8 all-gather.19
  233.1 6.7 reduce-scatter.2
  246.1 10.6 all-gather.21
  259.0 164.4 all-gather.23
  425.8 161.4 all-gather.25
  589.2 161.4 all-gather.27
  771.4 6.7 reduce-scatter.4
where the time goes:
time: 787 us
  waiting for transfers between devices  627 us (80%)
  blocking collectives  82.4 us (10%)
  matrix products  41.5 us (5%)
  other arithmetic  18 us (2%)
  between operations  14.8 us (2%)
    all_gather x2, waiting for transfers between devices, project_back(): lax.all_gather(weight, 'fs', axis=1, tiled=True)  214 us
    all_gather x1, waiting for transfers between devices, per_device(): lax.all_gather(channel_low[1], 'fs', axis=0, tiled=True)  153 us
    all_gather x1, waiting for transfers between devices, per_device(): lax.all_gather(channel_low[0], 'fs', axis=0, tiled=True)  149 us
    all_gather x1, waiting for transfers between devices, per_device(): lax.all_gather(mixer_low[0], 'fs', axis=0, tiled=True)  47.2 us
    all_gather x1, waiting for transfers between devices, per_device(): lax.all_gather(mixer_low[2], 'fs', axis=0, tiled=True)  46.9 us
    unnamed x1, blocking collectives  39.4 us
    dot_general x2, matrix products, project_back(): jnp.dot(hidden, lax.all_gather(weight, 'fs', axis=1, tiled=True), preferr...  25.6 us
    all_gather x1, blocking collectives, per_device(): lax.all_gather(down_scale, 'fs', axis=0, tiled=True)  21.1 us
  transfers between devices with their start and end apart: 11, of which 9 were waited for; matrix products, arithmetic and copies ran while one was open for 3% of the time, Pallas kernels for 0%

commit v1 on v0

--- a/solution.py
+++ b/solution.py
@@ -39,7 +39,7 @@
     product = (
         jnp.dot(
             hidden,
-            lax.all_gather(weight, "fs", axis=1, tiled=True),
+            jnp.concatenate(lax.all_gather(weight, "fs"), axis=1),
             preferred_element_type=jnp.float32,
         )
         * scale

time: 787 us -> 777 us (0.987)
  waiting for transfers between devices: 627 us -> 597 us
  local copies, waits for them, and re-layouts: 3.01 us -> 21.9 us
    all_gather x2, waiting for transfers between devices: 214 us -> 134 us  [project_back(): lax.all_gather(weight, 'fs')]
    all_gather x1, waiting for transfers between devices: 1.79 us -> 43.2 us  [per_device(): lax.all_gather(mixer_low[1], 'fs', axis=0, tiled=True)]
    reshape x0 -> x2, local copies, waits for them, and re-layouts: none -> 19.3 us  [project_back(): jnp.concatenate(lax.all_gather(weight, 'fs'), axis=1)]
    all_gather x1, waiting for transfers between devices: 149 us -> 161 us  [per_device(): lax.all_gather(channel_low[0], 'fs', axis=0, tiled=True)]
  transfers between devices with their start and end apart: 11 -> 11, of which waited for: 9 -> 8; matrix products, arithmetic and copies ran while one was open for 3% -> 7% of each run, Pallas kernels for 0% -> 0%
where the time goes in v1:
time: 777 us; the launch traced here: 776 us
  waiting for transfers between devices  597 us (77%)
  blocking collectives  83.5 us (11%)
  matrix products  40.2 us (5%)
  local copies, waits for them, and re-layouts  21.9 us (3%)
  other arithmetic  18.7 us (2%)
  between operations  14.7 us (2%)
    all_gather x1, waiting for transfers between devices, per_device(): lax.all_gather(channel_low[0], 'fs', axis=0, tiled=True)  161 us
    all_gather x1, waiting for transfers between devices, per_device(): lax.all_gather(channel_low[1], 'fs', axis=0, tiled=True)  153 us
    all_gather x2, waiting for transfers between devices, project_back(): lax.all_gather(weight, 'fs')  134 us
    all_gather x1, waiting for transfers between devices, per_device(): lax.all_gather(mixer_low[2], 'fs', axis=0, tiled=True)  46.7 us
    all_gather x1, waiting for transfers between devices, per_device(): lax.all_gather(mixer_low[0], 'fs', axis=0, tiled=True)  46.4 us
    all_gather x1, waiting for transfers between devices, per_device(): lax.all_gather(mixer_low[1], 'fs', axis=0, tiled=True)  43.2 us
    unnamed x1, blocking collectives  40 us
    dot_general x2, matrix products, project_back(): jnp.dot(hidden, jnp.concatenate(lax.all_gather(weight, 'fs'), axis=1), pr...  23.5 us
  transfers between devices with their start and end apart: 11, of which 8 were waited for; matrix products, arithmetic and copies ran while one was open for 7% of the time, Pallas kernels for 0%

profile of v1, /device:TPU:0, one launch (start us, length us, event | category | flops | bytes accessed | tf_op | source)
XLA Modules:
  0.0 776.2 jit_solution(6040730822287608760)
XLA Ops:
  6.5 1.9 convert_element_type.73
  8.5 0.0 all-gather.14.cloned.1.call-start
  8.5 1.4 fusion.4
  9.9 2.8 psum.14
  12.6 1.7 fusion.6
  14.5 0.0 all-gather.18.cloned.1.call-start
  14.5 0.7 convert_element_type.70
  15.3 0.0 all-gather.20.cloned.1.call-start
  15.3 0.7 convert_element_type.71
  16.1 0.0 all-gather.16.cloned.1.call-start
  16.2 0.7 convert_element_type.69
  17.0 0.6 dynamic-slice
  18.9 0.2 dynamic-update-slice
  19.1 0.2 dynamic-update-slice.1
  19.3 0.2 dynamic-update-slice.2
  19.6 0.3 dynamic-update-slice.3
  19.8 0.3 dynamic-update-slice.4
  20.1 40.0 %all-reduce.7 = (f32[512]{0:T(512)S(1)}, f32[512]{0:T(512)S(1)}, f32[512]{0:T(512)}, f32[2816]{0:T(1024)}, f32[2816]{0:T(1024)}) all-reduce(f32[512]{0:T(512)S(1)} %dynamic-update-slice.1, f32[512]{0:T(512)S(1)} %dynamic-update-slice.2, f32[512]{0:T(512)S(1)} %dynamic-update-slice, ...), channel_id=1, replica_groups=mesh['rep'=2,'fs'=8,'tp'=2] {'fs'}, use_global_device_ids=true, to_apply=%add.3 | all-reduce | flops 7168 | bytes 57344
  60.1 16.3 %all-gather.2 = f32[8,1,256]{2,1,0:T(1,128)S(1)} all-gather(f32[1,1,256]{2,1,0:T(1,128)S(1)} %bitcast.64), channel_id=1, replica_groups=mesh['rep'=2,'fs'=8,'tp'=2] {'fs'}, dimensions={0}, use_global_device_ids=true | all-gather | bytes 9216 | tf_op jit(solution)/shard_map/all_gather | solution.py:81
  76.4 0.6 fusion.30
  76.9 3.9 copy.23
  80.9 43.2 %all-gather.18.cloned.1.call-done = bf16[2048,512]{1,0:T(8,128)(2,1)} async-done(((bf16[256,512]{1,0:T(8,128)(2,1)}), bf16[2048,512]{1,0:T(8,128)(2,1)}) %all-gather.18.cloned.1.call-update) | async-done | bytes 2097168 | tf_op jit(solution)/shard_map/all_gather | solution.py:95
  124.1 2.9 convolution_multiply_fusion.5
  127.0 46.7 %all-gather.20.cloned.1.call-done = bf16[2048,512]{1,0:T(8,128)(2,1)} async-done(((bf16[256,512]{1,0:T(8,128)(2,1)}), bf16[2048,512]{1,0:T(8,128)(2,1)}) %all-gather.20.cloned.1.call-update) | async-done | bytes 2097168 | tf_op jit(solution)/shard_map/all_gather | solution.py:96
  173.7 3.3 fusion.12
  177.0 46.4 %all-gather.16.cloned.1.call-done = bf16[2048,512]{1,0:T(8,128)(2,1)} async-done(((bf16[256,512]{1,0:T(8,128)(2,1)}), bf16[2048,512]{1,0:T(8,128)(2,1)}) %all-gather.16.cloned.1.call-update) | async-done | bytes 2097168 | tf_op jit(solution)/shard_map/all_gather | solution.py:94
  223.4 6.2 fusion.2
  229.5 0.0 all-gather.30.cloned.1.call-start
  229.6 1.3 convert_element_type.82
  231.0 5.8 reduce-scatter.3.cloned.1.call-done
  236.9 1.4 fusion.8
  238.2 2.5 psum.15
  240.7 2.2 fusion.10
  242.9 0.0 all-gather.24.cloned.1.call-start
  243.0 1.3 convert_element_type.79
  244.3 0.0 all-gather.26.cloned.1.call-start
  244.3 3.1 convert_element_type.80
  247.4 0.0 reduce-scatter.5.cloned.1.call-start
  247.5 22.1 %all-gather.3 = f32[8,1,256]{2,1,0:T(1,128)S(1)} all-gather(f32[1,1,256]{2,1,0:T(1,128)S(1)} %bitcast.65), channel_id=1, replica_groups=mesh['rep'=2,'fs'=8,'tp'=2] {'fs'}, dimensions={0}, use_global_device_ids=true | all-gather | bytes 9216 | tf_op jit(solution)/shard_map/all_gather | solution.py:82
  269.6 0.1 slice_reduce_fusion.2
  269.7 133.9 %all-gather.30.cloned.1.call-done = bf16[22528,256]{1,0:T(8,128)(2,1)} async-done(((bf16[2816,256]{1,0:T(8,128)(2,1)}), bf16[22528,256]{1,0:T(8,128)(2,1)}) %all-gather.30.cloned.1.call-update) | async-done | bytes 11534352 | tf_op jit(solution)/shard_map/all_gather | solution.py:42
  403.6 15.3 %copy.24 = bf16[2816,8,256]{0,2,1:T(8,128)(2,1)} copy(bf16[2816,8,256]{2,0,1:T(8,128)(2,1)} %bitcast.55) | data formatting | bytes 23068672 | tf_op jit(solution)/shard_map/reshape | solution.py:42
  419.0 160.5 %all-gather.24.cloned.1.call-done = bf16[2048,2816]{1,0:T(8,128)(2,1)} async-done(((bf16[256,2816]{1,0:T(8,128)(2,1)}), bf16[2048,2816]{1,0:T(8,128)(2,1)}) %all-gather.24.cloned.1.call-update) | async-done | bytes 11534352 | tf_op jit(solution)/shard_map/all_gather | solution.py:108
  579.5 10.5 %convolution_multiply_fusion.1 = f32[320,2816]{1,0:T(8,128)} fusion(bf16[320,2048]{1,0:T(8,128)(2,1)} %all-gather.22.cloned.1.call-done, bf16[2048,2816]{1,0:T(8,128)(2,1)} %all-gather.24.cloned.1.call-done, f32[2816]{0:T(1024)S(1)} %copy-done.18), kind=kOutput, calls=%fused_computation.2 | convolution fusion | flops 3691888640 | bytes 16460800 | tf_op jit(solution)/shard_map/dot_general | solution.py:32
  590.0 153.0 %all-gather.26.cloned.1.call-done = bf16[2048,2816]{1,0:T(8,128)(2,1)} async-done(((bf16[256,2816]{1,0:T(8,128)(2,1)}), bf16[2048,2816]{1,0:T(8,128)(2,1)}) %all-gather.26.cloned.1.call-update) | async-done | bytes 11534352 | tf_op jit(solution)/shard_map/all_gather | solution.py:109
  743.1 17.4 %fusion.3 = bf16[320,2048]{1,0:T(8,128)(2,1)} fusion(bf16[2816,2048]{0,1:T(8,128)(2,1)} %bitcast.56, f32[2048]{0:T(1024)S(1)} %bitcast.60, bf16[320,2048]{1,0:T(8,128)(2,1)S(1)} %copy-done.15, bf16[2048,2816]{1,0:T(8,128)(2,1)} %all-gather.26.cloned.1.call-done, f32[320,2816]{1,0:T(8,128)} %convolution_multiply_fusion.1, f32[1,320,2816]{2,1,0:T(8,128)} %bitcast.66, ...), kind=kOutput, calls=%fused_computation.9 | convolution fusion | flops 7395000320 | bytes 32963584 | tf_op jit(solution)/shard_map/dot_general | solution.py:40
  760.5 7.0 reduce-scatter.5.cloned.1.call-done
  767.5 2.3 fusion.11
  (70 shorter events, 0.4 us)
Async XLA Ops:
  6.5 6.1 copy-start
  6.5 8.0 %copy-start.4 = (f32[256,512]{1,0:T(8,128)S(1)}, f32[256,512]{1,0:T(8,128)}, u32[]{:S(2)}) copy-start(f32[256,512]{1,0:T(8,128)} %param.23) | copy-start | bytes 1572868
  6.5 70.4 %all-gather.28.cloned.1.call-start = ((), (), s32[]{:S(2)}) async-start(), calls=%async_computation.11 | async-start | bytes 2359296 | tf_op jit(solution)/shard_map/all_gather | solution.py:42
  8.4 6.9 copy-start.5
  8.5 72.4 %all-gather.14.cloned.1.call-start = ((), (), s32[]{:S(2)}) async-start(), calls=%async_computation.2 | async-start | bytes 1966080 | tf_op jit(solution)/shard_map/all_gather | solution.py:16
  9.9 6.3 copy-start.6
  14.4 2.6 copy-start.22
  14.4 4.5 copy-start.19
  14.4 4.7 copy-start.20
  14.4 5.0 copy-start.21
  14.4 5.2 copy-start.10
  14.4 5.4 copy-start.11
  14.4 45.7 %copy-start.12 = (f32[256]{0:T(256)S(1)}, f32[256]{0:T(256)}, u32[]{:S(2)}) copy-start(f32[256]{0:T(256)} %param.30) | copy-start | bytes 3076
  14.4 61.9 %copy-start.8 = (f32[3,512]{1,0:T(4,128)S(1)}, f32[3,512]{1,0:T(4,128)}, u32[]{:S(2)}) copy-start(f32[3,512]{1,0:T(4,128)} %param.28) | copy-start | bytes 18436
  14.5 109.6 %all-gather.18.cloned.1.call-start = ((), (), s32[]{:S(2)}) async-start(), calls=%async_computation.4 | async-start | bytes 2359296 | tf_op jit(solution)/shard_map/all_gather | solution.py:95
  15.3 158.5 %all-gather.20.cloned.1.call-start = ((), (), s32[]{:S(2)}) async-start(), calls=%async_computation.5 | async-start | bytes 2359296 | tf_op jit(solution)/shard_map/all_gather | solution.py:96
  16.1 207.3 %all-gather.16.cloned.1.call-start = ((), (), s32[]{:S(2)}) async-start(), calls=%async_computation.3 | async-start | bytes 2359296 | tf_op jit(solution)/shard_map/all_gather | solution.py:94
  16.9 219.9 %reduce-scatter.3.cloned.1.call-start = ((), (), s32[]{:S(2)}) async-start(), calls=%async_computation.6 | async-start | bytes 1966080 | tf_op jit(solution)/shard_map/reduce_scatter | solution.py:48
  124.1 49.6 %copy-start.14 = (bf16[320,2048]{1,0:T(8,128)(2,1)S(1)}, bf16[320,2048]{1,0:T(8,128)(2,1)}, u32[]{:S(2)}) copy-start(bf16[320,2048]{1,0:T(8,128)(2,1)} %all-gather.14.cloned.1.call-done) | copy-start | bytes 3932164
  223.4 6.2 copy-start.2
  229.5 174.1 %all-gather.30.cloned.1.call-start = ((), (), s32[]{:S(2)}) async-start(), calls=%async_computation.12 | async-start | bytes 12976128 | tf_op jit(solution)/shard_map/all_gather | solution.py:42
  230.9 9.8 %copy-start.9 = (f32[1024]{0:T(1024)S(1)}, f32[1024]{0:T(1024)}, u32[]{:S(2)}) copy-start(f32[1024]{0:T(1024)} %param.31) | copy-start | bytes 12292
  231.0 12.0 %copy-start.3 = (f32[256,2816]{1,0:T(8,128)S(1)}, f32[256,2816]{1,0:T(8,128)}, u32[]{:S(2)}) copy-start(f32[256,2816]{1,0:T(8,128)} %param.32) | copy-start | bytes 8650756
  231.0 188.0 %all-gather.22.cloned.1.call-start = ((), (), s32[]{:S(2)}) async-start(), calls=%async_computation.7 | async-start | bytes 1966080 | tf_op jit(solution)/shard_map/all_gather | solution.py:16
  242.9 336.6 %all-gather.24.cloned.1.call-start = ((), (), s32[]{:S(2)}) async-start(), calls=%async_computation.8 | async-start | bytes 12976128 | tf_op jit(solution)/shard_map/all_gather | solution.py:108
  244.3 3.2 copy-start.13
  244.3 25.3 %copy-start.7 = (f32[3,2816]{1,0:T(4,128)S(1)}, f32[3,2816]{1,0:T(4,128)}, u32[]{:S(2)}) copy-start(f32[3,2816]{1,0:T(4,128)} %param.36) | copy-start | bytes 101380
  244.3 498.8 %all-gather.26.cloned.1.call-start = ((), (), s32[]{:S(2)}) async-start(), calls=%async_computation.9 | async-start | bytes 12976128 | tf_op jit(solution)/shard_map/all_gather | solution.py:109
  247.4 520.0 %reduce-scatter.5.cloned.1.call-start = ((), (), s32[]{:S(2)}) async-start(), calls=%async_computation.10 | async-start | bytes 1966080 | tf_op jit(solution)/shard_map/reduce_scatter | solution.py:48
  403.6 175.9 %copy-start.18 = (f32[2816]{0:T(1024)S(1)}, f32[2816]{0:T(1024)}, u32[]{:S(2)}) copy-start(f32[2816]{0:T(1024)} %get-tuple-element.11) | copy-start | bytes 33796
  579.5 163.6 %copy-start.15 = (bf16[320,2048]{1,0:T(8,128)(2,1)S(1)}, bf16[320,2048]{1,0:T(8,128)(2,1)}, u32[]{:S(2)}) copy-start(bf16[320,2048]{1,0:T(8,128)(2,1)} %all-gather.22.cloned.1.call-done) | copy-start | bytes 3932164
  579.5 163.6 %copy-start.16 = (f32[2816]{0:T(1024)S(1)}, f32[2816]{0:T(1024)}, u32[]{:S(2)}) copy-start(f32[2816]{0:T(1024)} %param.37) | copy-start | bytes 33796
  579.5 163.6 %copy-start.17 = (f32[2816]{0:T(1024)S(1)}, f32[2816]{0:T(1024)}, u32[]{:S(2)}) copy-start(f32[2816]{0:T(1024)} %get-tuple-element.12) | copy-start | bytes 33796
  743.1 24.4 %copy-start.1 = (bf16[320,1024]{1,0:T(8,128)(2,1)S(1)}, bf16[320,1024]{1,0:T(8,128)(2,1)}, u32[]{:S(2)}) copy-start(bf16[320,1024]{1,0:T(8,128)(2,1)} %reduce-scatter.3.cloned.1.call-done) | copy-start | bytes 1966084
Sparse Core Ops, SparseCore 0:
  9.5 52.4 all-gather.27
  63.5 8.0 all-gather.13
  73.8 50.2 all-gather.17
  126.1 47.6 all-gather.19
  175.7 47.6 all-gather.15
  229.7 7.1 reduce-scatter.2
  239.0 164.5 all-gather.29
  405.2 7.5 all-gather.21
  415.0 164.4 all-gather.23
  581.5 161.4 all-gather.25
  760.6 6.8 reduce-scatter.4
